TPU v7x, 256 devices: a 4x2x16 block of a 4x16x16 slice. The times are simulated.
256 devices in a mesh: grp: 2 (over y), sp: 32 (over z, core), tp: 4 (over x).
Axes of the slice: x: 4, y: 2, z: 16, core: 2. Of those that a mesh axis runs over, the one named last changes fastest.
The devices are a block of a 4x16x16 slice.
Arguments:
- carryover_vector: bfloat16 [16384, 2048], P(('grp', 'sp', 'tp')), parts along dimension 0, may hold values from -6 to 6
- channel_source_entries: bfloat16 [16384, 1024], P(('grp', 'sp'), 'tp'), parts along dimension 0, may hold values from -6 to 6
- final_modulation_vector: bfloat16 [16384, 1024], P(('grp', 'sp'), 'tp'), parts along dimension 0, may hold values from -54 to 54
- entering_basis_matrix: bfloat16 [16384, 512], P(('grp', 'sp'), 'tp'), parts along dimension 0, may hold values from -6 to 6
- readout_basis_matrix: bfloat16 [16384, 512], P(('grp', 'sp'), 'tp'), parts along dimension 0, may hold values from -6 to 6
- raw_stride_amount: float32 [16384, 16], P(('grp', 'sp'), 'tp'), parts along dimension 0, may hold values from -6 to 5
- extra_log_attenuation: float32 [16384, 16], P(('grp', 'sp'), 'tp'), parts along dimension 0, may hold values from -1.4 to 0
- channel_fading_rate: float32 [16], P('tp'), may hold values from 0 to 0.1, as said below
- channel_source_kernel: float32 [4, 1024], P(None, 'tp'), may hold values from -3 to 3
- entering_basis_kernel: float32 [4, 512], P(None, 'tp'), may hold values from -3 to 3
- readout_basis_kernel: float32 [4, 512], P(None, 'tp'), may hold values from -3 to 3
- modulated_rescaling_vector: float32 [1024], replicated, may hold values from 0.1 to 1.9
- blender_final_matrix: bfloat16 [1024, 2048], replicated, may hold values from -0.1875 to 0.1875
- specialist_rescaling_vector: float32 [2048], replicated, may hold values from 0.1 to 1.9
- specialist_gating_matrices: bfloat16 [64, 2048, 1024], P('sp', None, 'tp'), may hold values from -0.125 to 0.125
- widening_matrices: bfloat16 [64, 2048, 1024], P('sp', None, 'tp'), may hold values from -0.125 to 0.125
- contracting_matrices: bfloat16 [64, 1024, 2048], P('sp', 'tp'), may hold values from -0.1875 to 0.1875
- assigned_specialist_ids: int32 [16384, 2], P(('grp', 'sp')), parts along dimension 0, may hold values from 0 to 63, as said below
- specialist_choice_affinity: float32 [16384, 2], P(('grp', 'sp', 'tp')), parts along dimension 0, may hold values from -6 to 6
- cluster_chance: float32 [16384], P(('grp', 'sp', 'tp')), parts along dimension 0, may hold values from 0.25 to 1
Outputs:
- layer_out: bfloat16 [16384, 2048], P(('grp', 'sp', 'tp')), parts along dimension 0
There are 2 independent parts, one for each index of `grp`. A program takes and returns all parts, laid end to end along the dimension named above; an argument that names none is the same for every part. Nothing has to cross between parts.
Inputs may be any that keep to these rules, and one draw needn't show every extreme that they name: `assigned_specialist_ids`: each row names 2 different experts of one group: the experts g * 16 to (g + 1) * 16 - 1 for one g below 4. In each aligned block of 64 rows (the rows of one device) no expert is named by more than 4 rows, and every expert of one group, the same group in all blocks, is named by exactly 4 rows of every block. `channel_fading_rate`: positive.
All inputs are finite; a program needn't handle non-finite values.
Results may differ from a plain program's by a relative error of at most 0.015.
Values may be sent and summed in bfloat16 or wider, within the bound.
A program may use at most 64 MiB of HBM per device.

v0:
```python
import jax
import jax.numpy as jnp
from jax import lax
from jax.sharding import Mesh
from jax.sharding import PartitionSpec as P

HEAD_DIM = 64
STATE = 128
BLOCK = 64
SP = ("sp_0", "sp_1")
GRP_SP_TP = ("grp", "sp_0", "sp_1", "tp")
GRP_SP = ("grp", "sp_0", "sp_1")
EPS = 1e-06


def filled_with(x, identity):
    return jax.tree.map(
        lambda part, zero: jnp.zeros_like(part) + jnp.asarray(zero, part.dtype), x, identity
    )


def carried_in(x, axes, combine, identity):
    before = start = filled_with(x, identity)
    subtotal = x
    for axis in reversed(axes):
        size, index = (lax.axis_size(axis), lax.axis_index(axis))
        pieces = jax.tree.map(
            lambda part, kind: lax.all_gather(part.astype(kind), axis),
            subtotal,
            (jnp.bfloat16, jnp.bfloat16),
        )
        inside, subtotal = (start, start)
        for k in range(size):
            passed = k < index
            subtotal = combine(
                subtotal, jax.tree.map(lambda part, own: part[k].astype(own.dtype), pieces, x)
            )
            inside = jax.tree.map(lambda new, old: jnp.where(passed, new, old), subtotal, inside)
        before = combine(inside, before)
    return before


def from_behind(x, axis, by):
    size = lax.axis_size(axis)
    pairs = [(i, i + by) for i in range(size) if 0 <= i + by < size]
    return lax.ppermute(x, axis, pairs)


def for_sending(x):
    return jax.tree.map(lambda a: a.astype(jnp.bfloat16) if a.dtype == jnp.float32 else a, x)


def split_up(x, dim, size):
    shape = x.shape
    blocks = x.reshape(*shape[:dim], size, shape[dim] // size, *shape[dim + 1 :])
    return jnp.moveaxis(blocks, dim, 0)


def summed_on_arrival(x, axis, dim):
    size = lax.axis_size(axis)
    blocks = lax.all_to_all(split_up(x, dim, size), axis, 0, 0, tiled=True)
    return jnp.sum(blocks.astype(jnp.float32), axis=0)


def causal_conv(signal, earlier, weights):
    kernel_len = weights.shape[0]
    length = signal.shape[0]
    joined = jnp.concatenate([earlier, signal], axis=0).astype(jnp.float32)
    accumulated = jnp.zeros((length, signal.shape[1]), jnp.float32)
    for offset in range(kernel_len):
        accumulated = accumulated + weights[offset][None, :] * joined[offset : offset + length]
    return jax.nn.silu(accumulated)


def link_states(earlier, later):
    return (earlier[0] * later[0], earlier[1] * later[0][..., None, None] + later[1])


def device_states(scaled_in, log_attenuation, keys_b, queries_c, groups_here):
    length = scaled_in.shape[0]
    blocks = length // BLOCK
    per_group = scaled_in.shape[1] // groups_here
    scaled_in = scaled_in.reshape(blocks, BLOCK, groups_here, per_group, HEAD_DIM)
    log_attenuation = log_attenuation.reshape(blocks, BLOCK, groups_here, per_group)
    keys_b = keys_b.reshape(blocks, BLOCK, groups_here, STATE)
    queries_c = queries_c.reshape(blocks, BLOCK, groups_here, STATE)
    running = jnp.cumsum(log_attenuation, axis=1)
    lower_mask = jnp.tril(jnp.ones((BLOCK, BLOCK), dtype=bool))
    between = running[:, :, None] - running[:, None, :]
    decays = jnp.exp(jnp.where(lower_mask[None, :, :, None, None], between, -jnp.inf))
    scores = jnp.einsum("blgn,bsgn->blsg", queries_c, keys_b)
    inside = jnp.einsum("blsg,blsgr,bsgrp->blgrp", scores, decays, scaled_in)
    totals = running[:, -1]
    remain = jnp.exp(totals[:, None] - running)
    block_states = jnp.einsum("bsgn,bsgr,bsgrp->bgrpn", keys_b, remain, scaled_in)

    def advance(carried, pieces):
        return (carried * jnp.exp(pieces[1])[..., None, None] + pieces[0], carried)

    initial = jnp.zeros(block_states.shape[1:], jnp.float32)
    own_state, entering = lax.scan(advance, initial, (block_states, totals))
    own_decay = jnp.exp(jnp.sum(totals, axis=0))
    _, incoming = carried_in(
        (own_decay, own_state),
        SP,
        link_states,
        (jnp.ones_like(own_decay), jnp.zeros_like(own_state)),
    )
    preceding = jnp.exp(jnp.cumsum(totals, axis=0) - totals)
    entering = entering + preceding[..., None, None] * incoming[None]
    outside = jnp.einsum("blgn,bgrpn,blgr->blgrp", queries_c, entering, jnp.exp(running))
    return (inside + outside).reshape(length, -1)


def fetch_rows(tokens, sources):
    present = sources >= 0
    picked = jnp.take(tokens, jnp.maximum(sources, 0), axis=0)
    return jnp.where(present[:, None], picked, jnp.zeros_like(picked))


def slot_tables(chosen_ids, quarters, row_count, experts, capacity):
    picks = chosen_ids.shape[1]
    flat_ids = chosen_ids.reshape(quarters, row_count * picks)
    member = (flat_ids[..., None] == jnp.arange(experts, dtype=jnp.int32)).astype(jnp.int32)
    position = jnp.sum((jnp.cumsum(member, axis=1) - member) * member, axis=2)
    quarter_ids = jnp.arange(quarters, dtype=jnp.int32)[:, None]
    slot_index = flat_ids * (quarters * capacity) + quarter_ids * capacity + position
    token_index = (
        quarter_ids * row_count + jnp.arange(row_count * picks, dtype=jnp.int32)[None, :] // picks
    )
    sources = (
        jnp.full((experts * quarters * capacity,), -1, jnp.int32)
        .at[slot_index.reshape(-1)]
        .set(token_index.reshape(-1))
    )
    return (sources, position)


def per_device(
    carryover_vector,
    channel_source_entries,
    final_modulation_vector,
    entering_basis_matrix,
    readout_basis_matrix,
    raw_stride_amount,
    extra_log_attenuation,
    channel_fading_rate,
    channel_source_kernel,
    entering_basis_kernel,
    readout_basis_kernel,
    modulated_rescaling_vector,
    blender_final_matrix,
    specialist_rescaling_vector,
    specialist_gating_matrices,
    widening_matrices,
    contracting_matrices,
    assigned_specialist_ids,
    specialist_choice_affinity,
    cluster_chance,
):
    length = channel_source_entries.shape[0]
    row_count = carryover_vector.shape[0]
    model_width = carryover_vector.shape[1]
    heads_here = channel_fading_rate.shape[0]
    groups_here = entering_basis_matrix.shape[1] // STATE
    tp_index = lax.axis_index("tp")
    rim_rows = channel_source_kernel.shape[0] - 1
    neighbours = from_behind(
        (
            channel_source_entries[length - rim_rows :],
            entering_basis_matrix[length - rim_rows :],
            readout_basis_matrix[length - rim_rows :],
        ),
        SP,
        1,
    )
    inputs_x = causal_conv(channel_source_entries, neighbours[0], channel_source_kernel)
    keys_b = causal_conv(entering_basis_matrix, neighbours[1], entering_basis_kernel)
    queries_c = causal_conv(readout_basis_matrix, neighbours[2], readout_basis_kernel)
    channel_stride_amount = jax.nn.softplus(raw_stride_amount)
    log_attenuation = extra_log_attenuation - channel_fading_rate[None, :] * channel_stride_amount
    heads_x = inputs_x.reshape(length, heads_here, HEAD_DIM)
    mixed = device_states(
        heads_x * channel_stride_amount[:, :, None], log_attenuation, keys_b, queries_c, groups_here
    )
    gated = mixed * jax.nn.silu(final_modulation_vector.astype(jnp.float32))
    own_rows = lax.all_to_all(
        for_sending(gated), "tp", split_axis=0, concat_axis=1, tiled=True
    ).astype(gated.dtype)
    normed = (
        own_rows
        * lax.rsqrt(jnp.mean(own_rows * own_rows, axis=1, keepdims=True) + EPS)
        * modulated_rescaling_vector[None, :]
    ).astype(jnp.bfloat16)
    middle = (
        carryover_vector.astype(jnp.float32)
        + jnp.dot(normed, blender_final_matrix, preferred_element_type=jnp.float32)
    ).astype(jnp.bfloat16)
    middle_wide = middle.astype(jnp.float32)
    expert_input = (
        middle_wide
        * lax.rsqrt(jnp.mean(middle_wide * middle_wide, axis=1, keepdims=True) + EPS)
        * specialist_rescaling_vector[None, :]
    ).astype(jnp.bfloat16)
    sp_count = lax.axis_size(SP)
    local_experts = specialist_gating_matrices.shape[0]
    experts = sp_count * local_experts
    picks = assigned_specialist_ids.shape[1]
    capacity = 2 * row_count * picks // experts
    own_ids = lax.dynamic_slice_in_dim(assigned_specialist_ids, tp_index * row_count, row_count, 0)
    sources, position = slot_tables(own_ids, 1, row_count, experts, capacity)
    own_position = position[0]
    outgoing = fetch_rows(expert_input, sources).reshape(
        sp_count, local_experts, 1, capacity, model_width
    )
    received = lax.all_to_all(outgoing, SP, split_axis=0, concat_axis=0, tiled=True)
    arrived = lax.all_gather(received, "tp", axis=2, tiled=True)
    gate_value = jnp.einsum(
        "slqcd,ldf->slqcf", arrived, specialist_gating_matrices, preferred_element_type=jnp.float32
    )
    up_value = jnp.einsum(
        "slqcd,ldf->slqcf", arrived, widening_matrices, preferred_element_type=jnp.float32
    )
    hidden = (jax.nn.silu(gate_value) * up_value).astype(jnp.bfloat16)
    partial_value = jnp.einsum(
        "slqcf,lfd->slqcd", hidden, contracting_matrices, preferred_element_type=jnp.float32
    )
    width_total = summed_on_arrival(partial_value.astype(jnp.bfloat16), "tp", 2).astype(
        jnp.bfloat16
    )
    returned = lax.all_to_all(width_total, SP, split_axis=0, concat_axis=0, tiled=True)
    answers = returned.reshape(experts * capacity, model_width)
    own_slots = own_ids.reshape(-1) * capacity + own_position
    gathered = (
        jnp.take(answers, own_slots, axis=0)
        .reshape(row_count, picks, model_width)
        .astype(jnp.float32)
    )
    lifted = jnp.exp(specialist_choice_affinity)
    shares = cluster_chance[:, None] * lifted / jnp.sum(lifted, axis=1, keepdims=True)
    return (middle_wide + jnp.sum(shares[:, :, None] * gathered, axis=1)).astype(jnp.bfloat16)


def solution(mesh):
    finer = Mesh(
        mesh.devices.reshape(mesh.shape["grp"], 16, 2, mesh.shape["tp"]),
        ("grp", "sp_0", "sp_1", "tp"),
    )
    return jax.shard_map(
        per_device,
        mesh=finer,
        in_specs=(
            P(GRP_SP_TP, None),
            P(GRP_SP, "tp"),
            P(GRP_SP, "tp"),
            P(GRP_SP, "tp"),
            P(GRP_SP, "tp"),
            P(GRP_SP, "tp"),
            P(GRP_SP, "tp"),
            P("tp"),
            P(None, "tp"),
            P(None, "tp"),
            P(None, "tp"),
            P(),
            P(),
            P(),
            P(SP, None, "tp"),
            P(SP, None, "tp"),
            P(SP, "tp", None),
            P(GRP_SP, None),
            P(GRP_SP_TP, None),
            P(GRP_SP_TP),
        ),
        out_specs=P(GRP_SP_TP, None),
        check_vma=False,
    )
```

profile of v0, /device:TPU:33, one launch (start us, length us, event | category | flops | bytes accessed | tf_op | source)
XLA Modules:
  0.0 418.4 jit_solution(9210774802349872012)
XLA Ops:
  6.6 0.8 slice.211
  7.4 5.7 %collective-permute-start.2 = (bf16[3,256]{1,0:T(4,128)(2,1)S(1)}, bf16[3,256]{1,0:T(4,128)(2,1)S(1)}, u32[]{:S(2)}, u32[]{:S(2)}) collective-permute-start(bf16[3,256]{1,0:T(4,128)(2,1)S(1)} %slice.211), channel_id=1, source_target_pairs={{0,4},{4,8},{8,12},{12,16},{16,20},{20,24},{24,28},{28,32},{32,36}... | collective-permute-start | bytes 4616 | tf_op jit(solution)/shard_map/ppermute | solution.py:46
  13.8 1.9 collective-permute-start
  15.8 1.3 slice.202
  17.1 4.8 %collective-permute-start.1 = (bf16[3,128]{1,0:T(4,128)(2,1)}, bf16[3,128]{1,0:T(4,128)(2,1)}, u32[]{:S(2)}, u32[]{:S(2)}) collective-permute-start(bf16[3,128]{1,0:T(4,128)(2,1)} %slice.202), channel_id=1, source_target_pairs={{0,4},{4,8},{8,12},{12,16},{16,20},{20,24},{24,28},{28,32},{32,36}... | collective-permute-start | bytes 2312 | tf_op jit(solution)/shard_map/ppermute | solution.py:46
  21.9 0.8 fusion.93
  22.7 0.8 compare_select_fusion
  24.3 1.3 dynamic-slice
  26.5 0.8 slice_bitcast_fusion.24
  27.3 14.5 %all-reduce = bf16[8]{0:T(256)(128)(2,1)S(1)} all-reduce(bf16[8]{0:T(256)(128)(2,1)S(1)} %dynamic-update-slice), channel_id=2, replica_groups=mesh['grp'=2,'sp_0'=16,'sp_1'=2,'tp'=4] {'sp_1'}, use_global_device_ids=true, to_apply=%add | all-reduce | flops 8 | bytes 32
  42.5 0.8 broadcast_multiply_fusion
  46.8 0.9 maximum_convert_fusion.1
  47.8 0.9 maximum_convert_fusion
  49.6 5.7 %while.13 = (s32[]{:T(128)}, f32[1,4,64,128]{3,2,1,0:T(8,128)S(1)}, f32[4,1,4,64,128]{4,3,2,1,0:T(8,128)}, f32[4,1,4]{2,1,0:T(1,128)}, f32[4,1,4,64,128]{4,3,2,1,0:T(8,128)S(1)}, /*index=5*/s32[]{:T(128)}, s32[]{:T(128)}) while((s32[]{:T(128)}, f32[1,4,64,128]{3,2,1,0:T(8,128)S(1)}, f32[4,1,4,64,128]{4,3,2,1,0:T(8,128)}, ...), condition=%wide.region_2.3_spmd.clone, body=%wide.region_1.2_spmd.clone.sunk | while | flops 131075 | bytes 656016 | solution.py:101
  55.3 2.0 all-gather.1
  57.2 1.4 fusion.68
  59.5 1.1 scatter_custom_fusion
  60.6 25.0 %all_gather.22 = bf16[16,1,4]{2,1,0:T(2,128)(2,1)S(1)} all-gather(bf16[1,1,4]{2,1,0:T(2,128)(2,1)} %get-tuple-element.121), channel_id=1, replica_groups=mesh['grp'=2,'sp_0'=16,'sp_1'=2,'tp'=4] {'sp_0'}, dimensions={0}, use_global_device_ids=true | all-gather | bytes 136 | tf_op jit(solution)/shard_map/all_gather | solution.py:28
  86.2 0.8 slice_bitcast_fusion.20
  88.3 1.0 copy.79
  91.8 24.7 %all-gather.5.cloned.1.call-done = bf16[16,1,4,64,128]{4,3,2,1,0:T(8,128)(2,1)} async-done(((bf16[1,1,4,64,128]{4,3,2,1,0:T(8,128)(2,1)}), bf16[16,1,4,64,128]{4,3,2,1,0:T(8,128)(2,1)}) %all-gather.5.cloned.1.call-update) | async-done | bytes 1048592 | tf_op jit(solution)/shard_map/all_gather | solution.py:28
  116.5 1.7 fusion.65
  118.2 1.5 fusion.21
  119.6 1.0 fusion.22
  121.4 1.6 fusion.53
  123.0 4.0 all-to-all-start
  127.0 4.8 %all-to-all-done = bf16[4,64,256]{2,1,0:T(8,128)(2,1)S(1)} async-done(((bf16[4,64,256]{2,1,0:T(8,128)(2,1)}), bf16[4,64,256]{2,1,0:T(8,128)(2,1)S(1)}, u32[]{:S(2)}, u32[]{:S(2)}) %all-to-all-start) | async-done | bytes 131104 | tf_op jit(solution)/shard_map/all_to_all | solution.py:187
  132.1 3.2 multiply_reduce_fusion.1
  135.3 0.8 copy-done.1
  136.3 1.4 gather_fusion
  137.6 1.2 gather.13
  138.8 1.9 select_bitcast_fusion
  140.8 76.2 %all_to_all.28 = bf16[32,2,1,4,2048]{4,3,2,1,0:T(4,128)(2,1)S(1)} all-to-all(bf16[32,2,1,4,2048]{4,3,2,1,0:T(4,128)(2,1)S(1)} %select_bitcast_fusion), channel_id=1, replica_groups=mesh['grp'=2,'sp_0'=16,'sp_1'=2,'tp'=4] {'sp_0','sp_1'}, dimensions={0} | all-to-all | bytes 2097152 | tf_op jit(solution)/shard_map/all_to_all | solution.py:216
  217.0 1.6 copy.91
  218.6 44.0 %all-gather.7.cloned.1.call-done = bf16[32,2,4,4,2048]{4,0,3,2,1:T(8,128)(2,1)} async-done(((bf16[32,2,1,4,2048]{4,0,3,2,1:T(8,128)(2,1)}), bf16[32,2,4,4,2048]{4,0,3,2,1:T(8,128)(2,1)}) %all-gather.7.cloned.1.call-update) | async-done | bytes 4194320 | tf_op jit(solution)/shard_map/all_gather | solution.py:217
  262.6 4.1 fusion.9
  266.7 7.3 %convert_bitcast_fusion = bf16[4,32,2,1,4,2048]{5,1,4,0,2,3:T(8,128)(2,1)} fusion(bf16[2,256,2048]{2,1,0:T(8,128)(2,1)S(1)} %copy-done, bf16[32,2,4,4,2048]{4,0,3,2,1:T(8,128)(2,1)} %all-gather.7.cloned.1.call-done, bf16[2,2048,256]{2,1,0:T(8,128)(2,1)} %param.37, f32[32,2,4,4,256]{4,0,3,2,1:T(8,128)S(1)} %fusion.9), kind=kOutput, calls=%fused_computation.8 | convolution fusion | flops 2151153664 | bytes 13631488 | tf_op jit(solution)/shard_map/slqcf,lfd->slqcd/dot_general | solution.py:225
  274.0 2.5 copy.92
  276.5 51.3 %all_to_all.29 = bf16[4,32,2,1,4,2048]{5,1,4,2,3,0:T(8,128)(2,1)} all-to-all(bf16[4,32,2,1,4,2048]{5,1,4,2,3,0:T(8,128)(2,1)S(1)} %copy.92), channel_id=1, replica_groups=mesh['grp'=2,'sp_0'=16,'sp_1'=2,'tp'=4] {'tp'}, dimensions={0} | all-to-all | bytes 8388608 | tf_op jit(solution)/shard_map/all_to_all | solution.py:61
  327.8 3.1 reduce_sum.79
  330.9 1.9 copy.94
  332.8 14.3 %all-to-all-start.3 = ((bf16[32,2,1,4,2048]{4,3,1,2,0:T(4,128)(2,1)}), bf16[32,2,1,4,2048]{4,3,1,2,0:T(4,128)(2,1)}, u32[]{:S(2)}, u32[]{:S(2)}) async-start(bf16[32,2,1,4,2048]{4,3,1,2,0:T(4,128)(2,1)} %copy.94), calls=%async_computation.3 | async-start | bytes 2097152 | tf_op jit(solution)/shard_map/all_to_all | solution.py:231
  347.7 55.1 %all-to-all-done.3 = bf16[32,2,1,4,2048]{4,3,1,2,0:T(4,128)(2,1)} async-done(((bf16[32,2,1,4,2048]{4,3,1,2,0:T(4,128)(2,1)}), bf16[32,2,1,4,2048]{4,3,1,2,0:T(4,128)(2,1)}, u32[]{:S(2)}, u32[]{:S(2)}) %all-to-all-start.3) | async-done | bytes 1048608 | tf_op jit(solution)/shard_map/all_to_all | solution.py:231
  402.7 1.3 reshape.741
  404.1 1.7 gather_fusion.1
  405.8 1.4 gather.15
  407.2 2.5 multiply_reduce_fusion
  409.7 1.8 add_convert_fusion
  (111 shorter events, 19.2 us)
Async XLA Ops:
  6.5 260.2 %copy-start = (bf16[2,256,2048]{2,1,0:T(8,128)(2,1)S(1)}, bf16[2,256,2048]{2,1,0:T(8,128)(2,1)}, u32[]{:S(2)}) copy-start(bf16[2,256,2048]{2,1,0:T(8,128)(2,1)} %param.38) | copy-start | bytes 6291460
  6.6 109.9 %all-gather.5.cloned.1.call-start = ((), (), s32[]{:S(2)}) async-start(), calls=%async_computation.4 | async-start | bytes 1114112 | tf_op jit(solution)/shard_map/all_gather | solution.py:28
  7.4 40.4 %collective-permute-start.2 = (bf16[3,256]{1,0:T(4,128)(2,1)S(1)}, bf16[3,256]{1,0:T(4,128)(2,1)S(1)}, u32[]{:S(2)}, u32[]{:S(2)}) collective-permute-start(bf16[3,256]{1,0:T(4,128)(2,1)S(1)} %slice.211), channel_id=1, source_target_pairs={{0,4},{4,8},{8,12},{12,16},{16,20},{20,24},{24,28},{28,32},{32,36}... | collective-permute-start | bytes 4616 | tf_op jit(solution)/shard_map/ppermute | solution.py:46
  13.8 33.0 %collective-permute-start = (bf16[3,128]{1,0:T(4,128)(2,1)S(1)}, bf16[3,128]{1,0:T(4,128)(2,1)S(1)}, u32[]{:S(2)}, u32[]{:S(2)}) collective-permute-start(bf16[3,128]{1,0:T(4,128)(2,1)S(1)} %slice.193), channel_id=1, source_target_pairs={{0,4},{4,8},{8,12},{12,16},{16,20},{20,24},{24,28},{28,32},{32,36}... | collective-permute-start | bytes 2312 | tf_op jit(solution)/shard_map/ppermute | solution.py:46
  17.1 73.7 %collective-permute-start.1 = (bf16[3,128]{1,0:T(4,128)(2,1)}, bf16[3,128]{1,0:T(4,128)(2,1)}, u32[]{:S(2)}, u32[]{:S(2)}) collective-permute-start(bf16[3,128]{1,0:T(4,128)(2,1)} %slice.202), channel_id=1, source_target_pairs={{0,4},{4,8},{8,12},{12,16},{16,20},{20,24},{24,28},{28,32},{32,36}... | collective-permute-start | bytes 2312 | tf_op jit(solution)/shard_map/ppermute | solution.py:46
  24.3 24.4 %copy-start.6 = (f32[4,1,1,4]{3,2,1,0:T(1,128)}, f32[4,1,1,4]{3,2,1,0:T(1,128)S(1)}, u32[]{:S(2)}) copy-start(f32[4,1,1,4]{3,2,1,0:T(1,128)S(1)} %get-tuple-element.89) | copy-start | bytes 196
  43.2 3.5 copy-start.7
  43.9 4.9 %copy-start.11 = (s32[128]{0:T(128)}, s32[128]{0:T(128)S(1)}, u32[]{:S(2)}) copy-start(s32[128]{0:T(128)S(1)} %select_reduce_fusion) | copy-start | bytes 1540
  48.8 42.0 %copy-start.3 = (bf16[256,128]{1,0:T(8,128)(2,1)S(1)}, bf16[256,128]{1,0:T(8,128)(2,1)}, u32[]{:S(2)}) copy-start(bf16[256,128]{1,0:T(8,128)(2,1)} %param.26) | copy-start | bytes 196612
  91.7 40.4 %copy-start.2 = (bf16[64,2048]{1,0:T(8,128)(2,1)S(1)}, bf16[64,2048]{1,0:T(8,128)(2,1)}, u32[]{:S(2)}) copy-start(bf16[64,2048]{1,0:T(8,128)(2,1)} %param.22) | copy-start | bytes 786436
  91.7 40.4 %copy-start.10 = (f32[1024]{0:T(1024)S(1)}, f32[1024]{0:T(1024)}, u32[]{:S(2)}) copy-start(f32[1024]{0:T(1024)} %param.33) | copy-start | bytes 12292
  121.0 15.1 %copy-start.9 = (f32[2048]{0:T(1024)S(1)}, f32[2048]{0:T(1024)}, u32[]{:S(2)}) copy-start(f32[2048]{0:T(1024)} %param.35) | copy-start | bytes 24580
  123.0 8.8 %all-to-all-start = ((bf16[4,64,256]{2,1,0:T(8,128)(2,1)}), bf16[4,64,256]{2,1,0:T(8,128)(2,1)S(1)}, u32[]{:S(2)}, u32[]{:S(2)}) async-start(bf16[4,64,256]{2,1,0:T(8,128)(2,1)} %bitcast.53), calls=%async_computation | async-start | bytes 262144 | tf_op jit(solution)/shard_map/all_to_all | solution.py:187
  127.0 135.6 %all-gather.7.cloned.1.call-start = ((), (), s32[]{:S(2)}) async-start(), calls=%async_computation.5 | async-start | bytes 5242880 | tf_op jit(solution)/shard_map/all_gather | solution.py:217
  135.3 0.8 copy-start.1
  136.2 2.6 copy-start.4
  136.2 2.6 copy-start.5
  327.8 19.3 %copy-start.12 = (s32[128]{0:T(128)S(1)}, s32[128]{0:T(128)}, u32[]{:S(2)}) copy-start(s32[128]{0:T(128)} %copy-done.11) | copy-start | bytes 1540
  327.8 19.5 %copy-start.8 = (s32[64,2]{0,1:T(2,128)S(1)}, s32[64,2]{0,1:T(2,128)}, u32[]{:S(2)}) copy-start(s32[64,2]{0,1:T(2,128)} %copy-done.7) | copy-start | bytes 1540
  327.8 19.7 %copy-start.13 = (f32[64,2]{0,1:T(2,128)S(1)}, f32[64,2]{0,1:T(2,128)}, u32[]{:S(2)}) copy-start(f32[64,2]{0,1:T(2,128)} %param.40) | copy-start | bytes 1540
  327.8 19.7 %copy-start.15 = (f32[64]{0:T(128)S(1)}, f32[64]{0:T(128)}, u32[]{:S(2)}) copy-start(f32[64]{0:T(128)} %param.41) | copy-start | bytes 772
  327.8 19.8 %copy-start.14 = (s32[128]{0:T(128)S(1)}, s32[128]{0:T(128)}, u32[]{:S(2)}) copy-start(s32[128]{0:T(128)} %fusion.70) | copy-start | bytes 1540
  332.8 69.9 %all-to-all-start.3 = ((bf16[32,2,1,4,2048]{4,3,1,2,0:T(4,128)(2,1)}), bf16[32,2,1,4,2048]{4,3,1,2,0:T(4,128)(2,1)}, u32[]{:S(2)}, u32[]{:S(2)}) async-start(bf16[32,2,1,4,2048]{4,3,1,2,0:T(4,128)(2,1)} %copy.94), calls=%async_computation.3 | async-start | bytes 2097152 | tf_op jit(solution)/shard_map/all_to_all | solution.py:231
Sparse Core Ops, SparseCore 0:
  58.8 57.6 all-gather.4
  218.7 43.8 all-gather.6
where the time goes:
time: 420 us; the launch traced here: 418 us
  blocking collectives  169 us (40%)
  waiting for transfers between devices  129 us (31%)
  starting transfers between devices  30.8 us (7%)
  local copies, waits for them, and re-layouts  29.3 us (7%)
  other arithmetic  28.5 us (7%)
  matrix products  17.5 us (4%)
  between operations  14.6 us (3%)
    all_to_all x1, blocking collectives, per_device(): lax.all_to_all(outgoing, SP, split_axis=0, concat_axis=0, tiled=True)  76.2 us
    all_to_all x1, waiting for transfers between devices, per_device(): lax.all_to_all(width_total, SP, split_axis=0, concat_axis=0, tiled=True)  55.1 us
    all_to_all x1, blocking collectives, summed_on_arrival(): blocks = lax.all_to_all(split_up(x, dim, size), axis, 0, 0, tiled=True)  51.3 us
    all_gather x1, waiting for transfers between devices, per_device(): arrived = lax.all_gather(received, 'tp', axis=2, tiled=True)  44 us
    all_gather x2, blocking collectives, carried_in(): lax.all_gather(part.astype(kind), axis)  26.9 us
    all_gather x1, waiting for transfers between devices, carried_in(): lax.all_gather(part.astype(kind), axis)  24.7 us
    unnamed x1, blocking collectives  14.5 us
    all_to_all x1, starting transfers between devices, per_device(): lax.all_to_all(width_total, SP, split_axis=0, concat_axis=0, tiled=True)  14.3 us
  transfers between devices with their start and end apart: 7, of which 4 were waited for; matrix products, arithmetic and copies ran while one was open for 7% of the time, Pallas kernels for 0%

commit v1 on v0

--- a/solution.py
+++ b/solution.py
@@ -214,7 +214,21 @@
         sp_count, local_experts, 1, capacity, model_width
     )
     received = lax.all_to_all(outgoing, SP, split_axis=0, concat_axis=0, tiled=True)
-    arrived = lax.all_gather(received, "tp", axis=2, tiled=True)
+    ways, here, hop = (lax.axis_size("tp"), lax.axis_index("tp"), received.shape[2])
+    dims = [n * ways if d == 2 else n for d, n in enumerate(received.shape)]
+    full = lax.dynamic_update_slice_in_dim(
+        jnp.zeros(dims, received.dtype), received, here * hop, axis=2
+    )
+    going_up = going_down = received
+    for far in range(1, ways // 2 + 1):
+        going_up = lax.ppermute(going_up, "tp", [(d, (d + 1) % ways) for d in range(ways)])
+        full = lax.dynamic_update_slice_in_dim(full, going_up, (here - far) % ways * hop, axis=2)
+        if 2 * far < ways:
+            going_down = lax.ppermute(going_down, "tp", [(d, (d - 1) % ways) for d in range(ways)])
+            full = lax.dynamic_update_slice_in_dim(
+                full, going_down, (here + far) % ways * hop, axis=2
+            )
+    arrived = full
     gate_value = jnp.einsum(
         "slqcd,ldf->slqcf", arrived, specialist_gating_matrices, preferred_element_type=jnp.float32
     )

time: 420 us -> 416 us (level)
  local copies, waits for them, and re-layouts: 29.3 us -> 35.2 us
    all_gather x1 -> x0, waiting for transfers between devices: 44 us -> none  [per_device(): arrived = lax.all_gather(received, 'tp', axis=2, tiled=True)]
    ppermute x0 -> x3, waiting for transfers between devices: none -> 42.7 us  [the longest x2 42.7 us: per_device(): lax.ppermute(going_up, 'tp', [(d, (d + 1) % ways) for d in range(ways)])]
    all_to_all x1, starting transfers between devices: 14.3 us -> 7.78 us  [per_device(): lax.all_to_all(width_total, SP, split_axis=0, concat_axis=0, tiled=True)]
    dynamic_update_slice x0 -> x4, local copies, waits for them, and re-layouts: none -> 5.01 us  [the longest x2 2.5 us: per_device(): lax.dynamic_update_slice_in_dim(full, going_up, (here - far) % ways * hop...]
  transfers between devices with their start and end apart: 7 -> 9, of which waited for: 4 -> 5; matrix products, arithmetic and copies ran while one was open for 7% -> 8% of each run, Pallas kernels for 0% -> 0%
where the time goes in v1:
time: 416 us; the launch traced here: 415 us
  blocking collectives  167 us (40%)
  waiting for transfers between devices  128 us (31%)
  local copies, waits for them, and re-layouts  35.2 us (8%)
  other arithmetic  28.5 us (7%)
  starting transfers between devices  27.2 us (7%)
  matrix products  14.7 us (4%)
  between operations  14.6 us (4%)
    all_to_all x1, blocking collectives, per_device(): lax.all_to_all(outgoing, SP, split_axis=0, concat_axis=0, tiled=True)  76 us
    all_to_all x1, waiting for transfers between devices, per_device(): lax.all_to_all(width_total, SP, split_axis=0, concat_axis=0, tiled=True)  55.2 us
    all_to_all x1, blocking collectives, summed_on_arrival(): blocks = lax.all_to_all(split_up(x, dim, size), axis, 0, 0, tiled=True)  49.9 us
    ppermute x2, waiting for transfers between devices, per_device(): lax.ppermute(going_up, 'tp', [(d, (d + 1) % ways) for d in range(ways)])  42.7 us
    all_gather x2, blocking collectives, carried_in(): lax.all_gather(part.astype(kind), axis)  26.5 us
    all_gather x1, waiting for transfers between devices, carried_in(): lax.all_gather(part.astype(kind), axis)  25.3 us
    unnamed x1, blocking collectives  14.5 us
    ppermute x3, starting transfers between devices, from_behind(): return lax.ppermute(x, axis, pairs)  12.5 us
  transfers between devices with their start and end apart: 9, of which 5 were waited for; matrix products, arithmetic and copies ran while one was open for 8% of the time, Pallas kernels for 0%

profile of v1, /device:TPU:33, one launch (start us, length us, event | category | flops | bytes accessed | tf_op | source)
XLA Modules:
  0.0 415.1 jit_solution(1676475671434838788)
XLA Ops:
  6.6 0.8 slice.211
  7.4 5.7 %collective-permute-start.2 = (bf16[3,256]{1,0:T(4,128)(2,1)S(1)}, bf16[3,256]{1,0:T(4,128)(2,1)S(1)}, u32[]{:S(2)}, u32[]{:S(2)}) collective-permute-start(bf16[3,256]{1,0:T(4,128)(2,1)S(1)} %slice.211), channel_id=1, source_target_pairs={{0,4},{4,8},{8,12},{12,16},{16,20},{20,24},{24,28},{28,32},{32,36}... | collective-permute-start | bytes 4616 | tf_op jit(solution)/shard_map/ppermute | solution.py:46
  13.8 1.9 collective-permute-start
  15.8 1.3 slice.202
  17.1 4.8 %collective-permute-start.1 = (bf16[3,128]{1,0:T(4,128)(2,1)}, bf16[3,128]{1,0:T(4,128)(2,1)}, u32[]{:S(2)}, u32[]{:S(2)}) collective-permute-start(bf16[3,128]{1,0:T(4,128)(2,1)} %slice.202), channel_id=1, source_target_pairs={{0,4},{4,8},{8,12},{12,16},{16,20},{20,24},{24,28},{28,32},{32,36}... | collective-permute-start | bytes 2312 | tf_op jit(solution)/shard_map/ppermute | solution.py:46
  21.9 0.8 fusion.90
  24.4 1.3 dynamic-slice
  27.4 14.5 %all-reduce = bf16[8]{0:T(256)(128)(2,1)S(1)} all-reduce(bf16[8]{0:T(256)(128)(2,1)S(1)} %dynamic-update-slice), channel_id=2, replica_groups=mesh['grp'=2,'sp_0'=16,'sp_1'=2,'tp'=4] {'sp_1'}, use_global_device_ids=true, to_apply=%add | all-reduce | flops 8 | bytes 32
  47.0 0.9 maximum_convert_fusion.1
  47.9 0.9 maximum_convert_fusion
  49.8 5.7 %while.13 = (s32[]{:T(128)}, f32[1,4,64,128]{3,2,1,0:T(8,128)S(1)}, f32[4,1,4,64,128]{4,3,2,1,0:T(8,128)}, f32[4,1,4]{2,1,0:T(1,128)}, f32[4,1,4,64,128]{4,3,2,1,0:T(8,128)S(1)}, /*index=5*/s32[]{:T(128)}, s32[]{:T(128)}) while((s32[]{:T(128)}, f32[1,4,64,128]{3,2,1,0:T(8,128)S(1)}, f32[4,1,4,64,128]{4,3,2,1,0:T(8,128)}, ...), condition=%wide.region_2.3_spmd.clone, body=%wide.region_1.2_spmd.clone.sunk | while | flops 131075 | bytes 656016 | solution.py:101
  55.4 2.0 all-gather.1
  57.4 1.4 fusion.65
  59.6 1.1 scatter_custom_fusion
  60.8 24.6 %all_gather.19 = bf16[16,1,4]{2,1,0:T(2,128)(2,1)S(1)} all-gather(bf16[1,1,4]{2,1,0:T(2,128)(2,1)} %get-tuple-element.121), channel_id=1, replica_groups=mesh['grp'=2,'sp_0'=16,'sp_1'=2,'tp'=4] {'sp_0'}, dimensions={0}, use_global_device_ids=true | all-gather | bytes 136 | tf_op jit(solution)/shard_map/all_gather | solution.py:28
  85.8 0.8 slice_bitcast_fusion.20
  87.9 1.0 copy.83
  91.4 25.3 %all-gather.4.cloned.1.call-done = bf16[16,1,4,64,128]{4,3,2,1,0:T(8,128)(2,1)} async-done(((bf16[1,1,4,64,128]{4,3,2,1,0:T(8,128)(2,1)}), bf16[16,1,4,64,128]{4,3,2,1,0:T(8,128)(2,1)}) %all-gather.4.cloned.1.call-update) | async-done | bytes 1048592 | tf_op jit(solution)/shard_map/all_gather | solution.py:28
  116.7 1.7 fusion.62
  118.3 1.5 fusion.15
  119.8 1.0 fusion.16
  121.6 1.6 fusion.50
  123.2 4.2 %all-to-all-start = ((bf16[4,64,256]{2,1,0:T(8,128)(2,1)}), bf16[4,64,256]{2,1,0:T(8,128)(2,1)S(1)}, u32[]{:S(2)}, u32[]{:S(2)}) async-start(bf16[4,64,256]{2,1,0:T(8,128)(2,1)} %bitcast.53), calls=%async_computation | async-start | bytes 262144 | tf_op jit(solution)/shard_map/all_to_all | solution.py:187
  127.4 4.8 %all-to-all-done = bf16[4,64,256]{2,1,0:T(8,128)(2,1)S(1)} async-done(((bf16[4,64,256]{2,1,0:T(8,128)(2,1)}), bf16[4,64,256]{2,1,0:T(8,128)(2,1)S(1)}, u32[]{:S(2)}, u32[]{:S(2)}) %all-to-all-start) | async-done | bytes 131104 | tf_op jit(solution)/shard_map/all_to_all | solution.py:187
  132.5 3.2 multiply_reduce_fusion.1
  136.7 1.4 gather_fusion
  138.0 1.2 gather.13
  139.3 1.9 fusion.17
  141.2 76.0 %all_to_all.28 = bf16[32,2,1,4,2048]{4,3,2,1,0:T(4,128)(2,1)S(1)} all-to-all(bf16[32,2,1,4,2048]{4,3,2,1,0:T(4,128)(2,1)S(1)} %fusion.17), channel_id=1, replica_groups=mesh['grp'=2,'sp_0'=16,'sp_1'=2,'tp'=4] {'sp_0','sp_1'}, dimensions={0} | all-to-all | bytes 2097152 | tf_op jit(solution)/shard_map/all_to_all | solution.py:216
  217.4 2.4 collective-permute-start.4
  219.8 22.8 %collective-permute-done.3 = bf16[32,2,1,4,2048]{4,3,2,1,0:T(4,128)(2,1)} collective-permute-done((bf16[32,2,1,4,2048]{4,3,2,1,0:T(4,128)(2,1)S(1)}, bf16[32,2,1,4,2048]{4,3,2,1,0:T(4,128)(2,1)}, u32[]{:S(2)}, u32[]{:S(2)}) %collective-permute-start.3) | collective-permute-done | bytes 1048608 | tf_op jit(solution)/shard_map/ppermute | solution.py:224
  243.8 1.9 copy_dynamic-update-slice_fusion.2
  245.7 1.9 copy_dynamic-update-slice_fusion.1
  247.6 19.8 %collective-permute-done.5 = bf16[32,2,1,4,2048]{4,3,2,1,0:T(4,128)(2,1)S(1)} collective-permute-done((bf16[32,2,1,4,2048]{4,3,2,1,0:T(4,128)(2,1)}, bf16[32,2,1,4,2048]{4,3,2,1,0:T(4,128)(2,1)S(1)}, u32[]{:S(2)}, u32[]{:S(2)}) %collective-permute-start.5) | collective-permute-done | bytes 1048608 | tf_op jit(solution)/shard_map/ppermute | solution.py:224
  268.1 1.9 copy-done.2
  270.0 1.3 fusion.9
  271.3 7.3 %convert_bitcast_fusion = bf16[4,32,2,1,4,2048]{5,1,4,0,2,3:T(8,128)(2,1)} fusion(bf16[2,256,2048]{2,1,0:T(8,128)(2,1)S(1)} %copy-done, f32[32,2,4,4,256]{4,0,3,2,1:T(8,128)S(1)} %fusion.9, bf16[32,2,4,4,2048]{4,0,3,2,1:T(8,128)(2,1)} %copy-done.2, bf16[2,2048,256]{2,1,0:T(8,128)(2,1)} %param.37), kind=kOutput, calls=%fused_computation.8 | convolution fusion | flops 2151153664 | bytes 13631488 | tf_op jit(solution)/shard_map/slqcf,lfd->slqcd/dot_general | solution.py:239
  278.6 2.5 copy.99
  281.1 49.9 %all_to_all.29 = bf16[4,32,2,1,4,2048]{5,1,4,2,3,0:T(8,128)(2,1)} all-to-all(bf16[4,32,2,1,4,2048]{5,1,4,2,3,0:T(8,128)(2,1)S(1)} %copy.99), channel_id=1, replica_groups=mesh['grp'=2,'sp_0'=16,'sp_1'=2,'tp'=4] {'tp'}, dimensions={0} | all-to-all | bytes 8388608 | tf_op jit(solution)/shard_map/all_to_all | solution.py:61
  331.0 3.1 reduce_sum.79
  334.1 1.8 copy.101
  335.9 7.8 %all-to-all-start.3 = ((bf16[32,2,1,4,2048]{4,3,1,2,0:T(4,128)(2,1)}), bf16[32,2,1,4,2048]{4,3,1,2,0:T(4,128)(2,1)}, u32[]{:S(2)}, u32[]{:S(2)}) async-start(bf16[32,2,1,4,2048]{4,3,1,2,0:T(4,128)(2,1)} %copy.101), calls=%async_computation.3 | async-start | bytes 2097152 | tf_op jit(solution)/shard_map/all_to_all | solution.py:245
  344.2 55.2 %all-to-all-done.3 = bf16[32,2,1,4,2048]{4,3,1,2,0:T(4,128)(2,1)} async-done(((bf16[32,2,1,4,2048]{4,3,1,2,0:T(4,128)(2,1)}), bf16[32,2,1,4,2048]{4,3,1,2,0:T(4,128)(2,1)}, u32[]{:S(2)}, u32[]{:S(2)}) %all-to-all-start.3) | async-done | bytes 1048608 | tf_op jit(solution)/shard_map/all_to_all | solution.py:245
  399.4 1.3 reshape.741
  400.7 1.7 gather_fusion.1
  402.5 1.4 gather.15
  403.8 2.5 multiply_reduce_fusion
  406.4 1.8 add_convert_fusion
  (122 shorter events, 24.4 us)
Async XLA Ops:
  6.5 264.7 %copy-start = (bf16[2,256,2048]{2,1,0:T(8,128)(2,1)S(1)}, bf16[2,256,2048]{2,1,0:T(8,128)(2,1)}, u32[]{:S(2)}) copy-start(bf16[2,256,2048]{2,1,0:T(8,128)(2,1)} %param.38) | copy-start | bytes 6291460
  6.6 110.1 %all-gather.4.cloned.1.call-start = ((), (), s32[]{:S(2)}) async-start(), calls=%async_computation.4 | async-start | bytes 1114112 | tf_op jit(solution)/shard_map/all_gather | solution.py:28
  7.4 40.5 %collective-permute-start.2 = (bf16[3,256]{1,0:T(4,128)(2,1)S(1)}, bf16[3,256]{1,0:T(4,128)(2,1)S(1)}, u32[]{:S(2)}, u32[]{:S(2)}) collective-permute-start(bf16[3,256]{1,0:T(4,128)(2,1)S(1)} %slice.211), channel_id=1, source_target_pairs={{0,4},{4,8},{8,12},{12,16},{16,20},{20,24},{24,28},{28,32},{32,36}... | collective-permute-start | bytes 4616 | tf_op jit(solution)/shard_map/ppermute | solution.py:46
  13.8 33.1 %collective-permute-start = (bf16[3,128]{1,0:T(4,128)(2,1)S(1)}, bf16[3,128]{1,0:T(4,128)(2,1)S(1)}, u32[]{:S(2)}, u32[]{:S(2)}) collective-permute-start(bf16[3,128]{1,0:T(4,128)(2,1)S(1)} %slice.193), channel_id=1, source_target_pairs={{0,4},{4,8},{8,12},{12,16},{16,20},{20,24},{24,28},{28,32},{32,36}... | collective-permute-start | bytes 2312 | tf_op jit(solution)/shard_map/ppermute | solution.py:46
  17.1 73.3 %collective-permute-start.1 = (bf16[3,128]{1,0:T(4,128)(2,1)}, bf16[3,128]{1,0:T(4,128)(2,1)}, u32[]{:S(2)}, u32[]{:S(2)}) collective-permute-start(bf16[3,128]{1,0:T(4,128)(2,1)} %slice.202), channel_id=1, source_target_pairs={{0,4},{4,8},{8,12},{12,16},{16,20},{20,24},{24,28},{28,32},{32,36}... | collective-permute-start | bytes 2312 | tf_op jit(solution)/shard_map/ppermute | solution.py:46
  24.3 24.5 %copy-start.7 = (f32[4,1,1,4]{3,2,1,0:T(1,128)}, f32[4,1,1,4]{3,2,1,0:T(1,128)S(1)}, u32[]{:S(2)}) copy-start(f32[4,1,1,4]{3,2,1,0:T(1,128)S(1)} %get-tuple-element.89) | copy-start | bytes 196
  43.3 3.6 copy-start.8
  44.0 4.9 %copy-start.12 = (s32[128]{0:T(128)}, s32[128]{0:T(128)S(1)}, u32[]{:S(2)}) copy-start(s32[128]{0:T(128)S(1)} %select_reduce_fusion) | copy-start | bytes 1540
  48.9 41.4 %copy-start.4 = (bf16[256,128]{1,0:T(8,128)(2,1)S(1)}, bf16[256,128]{1,0:T(8,128)(2,1)}, u32[]{:S(2)}) copy-start(bf16[256,128]{1,0:T(8,128)(2,1)} %param.26) | copy-start | bytes 196612
  91.3 41.2 %copy-start.3 = (bf16[64,2048]{1,0:T(8,128)(2,1)S(1)}, bf16[64,2048]{1,0:T(8,128)(2,1)}, u32[]{:S(2)}) copy-start(bf16[64,2048]{1,0:T(8,128)(2,1)} %param.22) | copy-start | bytes 786436
  91.3 41.2 %copy-start.11 = (f32[1024]{0:T(1024)S(1)}, f32[1024]{0:T(1024)}, u32[]{:S(2)}) copy-start(f32[1024]{0:T(1024)} %param.33) | copy-start | bytes 12292
  121.2 15.3 %copy-start.10 = (f32[2048]{0:T(1024)S(1)}, f32[2048]{0:T(1024)}, u32[]{:S(2)}) copy-start(f32[2048]{0:T(1024)} %param.35) | copy-start | bytes 24580
  123.2 9.1 %all-to-all-start = ((bf16[4,64,256]{2,1,0:T(8,128)(2,1)}), bf16[4,64,256]{2,1,0:T(8,128)(2,1)S(1)}, u32[]{:S(2)}, u32[]{:S(2)}) async-start(bf16[4,64,256]{2,1,0:T(8,128)(2,1)} %bitcast.53), calls=%async_computation | async-start | bytes 262144 | tf_op jit(solution)/shard_map/all_to_all | solution.py:187
  135.7 0.8 copy-start.1
  136.6 2.6 copy-start.5
  136.7 2.6 copy-start.6
  217.1 25.5 %collective-permute-start.3 = (bf16[32,2,1,4,2048]{4,3,2,1,0:T(4,128)(2,1)S(1)}, bf16[32,2,1,4,2048]{4,3,2,1,0:T(4,128)(2,1)}, u32[]{:S(2)}, u32[]{:S(2)}) collective-permute-start(bf16[32,2,1,4,2048]{4,3,2,1,0:T(4,128)(2,1)S(1)} %all_to_all.28), channel_id=1, source_target_pairs={{0,1},{1,2},{2,3},{3,0},{4,5},{5,6},{6,7},{7,4},{8,9},{9,10},{10,1... | collective-permute-start | bytes 3145736 | tf_op jit(solution)/shard_map/ppermute | solution.py:224
  217.4 28.3 %collective-permute-start.4 = (bf16[32,2,1,4,2048]{4,3,2,1,0:T(4,128)(2,1)S(1)}, bf16[32,2,1,4,2048]{4,3,2,1,0:T(4,128)(2,1)}, u32[]{:S(2)}, u32[]{:S(2)}) collective-permute-start(bf16[32,2,1,4,2048]{4,3,2,1,0:T(4,128)(2,1)S(1)} %all_to_all.28), channel_id=1, source_target_pairs={{0,3},{1,0},{2,1},{3,2},{4,7},{5,4},{6,5},{7,6},{8,11},{9,8},{10,9... | collective-permute-start | bytes 3145736 | tf_op jit(solution)/shard_map/ppermute | solution.py:227
  242.7 24.8 %collective-permute-start.5 = (bf16[32,2,1,4,2048]{4,3,2,1,0:T(4,128)(2,1)}, bf16[32,2,1,4,2048]{4,3,2,1,0:T(4,128)(2,1)S(1)}, u32[]{:S(2)}, u32[]{:S(2)}) collective-permute-start(bf16[32,2,1,4,2048]{4,3,2,1,0:T(4,128)(2,1)} %collective-permute-done.3), channel_id=1, source_target_pairs={{0,1},{1,2},{2,3},{3,0},{4,5},{5,6},{6,7},{7,4},{8,9},{9,10},{10,1... | collective-permute-start | bytes 3145736 | tf_op jit(solution)/shard_map/ppermute | solution.py:224
  243.2 26.8 %copy-start.17 = (bf16[2,2048,256]{2,1,0:T(8,128)(2,1)S(1)}, bf16[2,2048,256]{2,1,0:T(8,128)(2,1)}, u32[]{:S(2)}) copy-start(bf16[2,2048,256]{2,1,0:T(8,128)(2,1)} %param.36) | copy-start | bytes 6291460
  268.1 1.9 copy-start.2
  331.0 12.7 %copy-start.13 = (s32[128]{0:T(128)S(1)}, s32[128]{0:T(128)}, u32[]{:S(2)}) copy-start(s32[128]{0:T(128)} %copy-done.12) | copy-start | bytes 1540
  331.0 13.0 %copy-start.9 = (s32[64,2]{0,1:T(2,128)S(1)}, s32[64,2]{0,1:T(2,128)}, u32[]{:S(2)}) copy-start(s32[64,2]{0,1:T(2,128)} %copy-done.8) | copy-start | bytes 1540
  331.0 13.1 %copy-start.14 = (f32[64,2]{0,1:T(2,128)S(1)}, f32[64,2]{0,1:T(2,128)}, u32[]{:S(2)}) copy-start(f32[64,2]{0,1:T(2,128)} %param.40) | copy-start | bytes 1540
  331.0 13.1 %copy-start.16 = (f32[64]{0:T(128)S(1)}, f32[64]{0:T(128)}, u32[]{:S(2)}) copy-start(f32[64]{0:T(128)} %param.41) | copy-start | bytes 772
  331.0 13.2 %copy-start.15 = (s32[128]{0:T(128)S(1)}, s32[128]{0:T(128)}, u32[]{:S(2)}) copy-start(s32[128]{0:T(128)} %fusion.67) | copy-start | bytes 1540
  335.9 63.5 %all-to-all-start.3 = ((bf16[32,2,1,4,2048]{4,3,1,2,0:T(4,128)(2,1)}), bf16[32,2,1,4,2048]{4,3,1,2,0:T(4,128)(2,1)}, u32[]{:S(2)}, u32[]{:S(2)}) async-start(bf16[32,2,1,4,2048]{4,3,1,2,0:T(4,128)(2,1)} %copy.101), calls=%async_computation.3 | async-start | bytes 2097152 | tf_op jit(solution)/shard_map/all_to_all | solution.py:245
Sparse Core Ops, SparseCore 0:
  59.0 57.6 all-gather.3
